TPU v7x, 32 devices: a whole 2x2x4 slice. The times are simulated.
32 devices in a mesh: grp: 2 (over x), tp: 16 (over z, y, core).
Axes of the slice: x: 2, y: 2, z: 4, core: 2. Of those that a mesh axis runs over, the one named last changes fastest.
Arguments:
- tokens: bfloat16 [160, 2048], P('grp', 'tp'), parts along dimension 0, may hold values from -6 to 6
- lengths: int32 [160], P('grp'), parts along dimension 0, may hold values from 1 to 4096, 81920 in all
- cell_memory: float32 [2, 160, 2048, 256], P(None, 'grp', 'tp'), parts along dimension 1, may hold values from -0.6 to 0.6
- key_sums: float32 [2, 160, 2048], P(None, 'grp', 'tp'), parts along dimension 1, may hold values from -3 to 3
- stabilizer: float32 [2, 160, 8], P(None, 'grp'), parts along dimension 1, may hold values from -3 to 1
- norm_gain: bfloat16 [2, 2048], replicated, may hold values from 0.099609375 to 1.8984375
- query_weight: bfloat16 [2, 2048, 2048], P(None, None, 'tp'), may hold values from -0.125 to 0.125
- key_weight: bfloat16 [2, 2048, 2048], P(None, None, 'tp'), may hold values from -0.125 to 0.125
- value_weight: bfloat16 [2, 2048, 2048], P(None, None, 'tp'), may hold values from -0.125 to 0.125
- outgate_weight: bfloat16 [2, 2048, 2048], P(None, None, 'tp'), may hold values from -0.125 to 0.125
- ingate_weight: bfloat16 [2, 2048, 8], replicated, may hold values from -0.125 to 0.125
- forget_weight: bfloat16 [2, 2048, 8], replicated, may hold values from -0.125 to 0.125
- ingate_bias: float32 [2, 8], replicated, may hold values from -3 to 3
- forget_bias: float32 [2, 8], replicated, may hold values from -1 to 4
- forget_slope: float32 [2, 8], replicated, may hold values from -3 to 3
- head_gain: bfloat16 [2, 2048], P(None, 'tp'), may hold values from 0.099609375 to 1.8984375
- output_weight: bfloat16 [2, 2048, 2048], P(None, None, 'tp'), may hold values from -0.125 to 0.125
Outputs:
- new_tokens: bfloat16 [160, 2048], P('grp', 'tp'), parts along dimension 0
- new_memory: float32 [2, 160, 2048, 256], P(None, 'grp', 'tp'), parts along dimension 1
- new_key_sums: float32 [2, 160, 2048], P(None, 'grp', 'tp'), parts along dimension 1
- new_stabilizer: float32 [2, 160, 8], P(None, 'grp'), parts along dimension 1
There are 2 independent parts, one for each index of `grp`. A program takes and returns all parts, laid end to end along the dimension named above; an argument that names none is the same for every part. Nothing has to cross between parts.
Inputs may be any that keep to these rules, and one draw needn't show every extreme that they name: Each part's 80 lengths sum to 81920, and the largest is exactly 4096.
All inputs are finite; a program needn't handle non-finite values.
Results may differ from a plain program's by a relative error of at most 0.018.
Values may be sent and summed in bfloat16 or wider, within the bound.
A program may use at most 128 MiB of HBM per device.

v0:
```python
import jax
import jax.numpy as jnp
from jax import lax
from jax.sharding import PartitionSpec as P

HEADS = 8
HEAD = 256
MAXLEN = 4096
EPS = 1e-05


def from_partner(value, axis, stride):
    mask = 2**stride
    pairs = [(source, source ^ mask) for source in range(lax.axis_size(axis))]
    return lax.ppermute(value, axis, pairs)


def body(
    tokens,
    lengths,
    cell_memory,
    key_sums,
    stabilizer,
    norm_gain,
    query_weight,
    key_weight,
    value_weight,
    outgate_weight,
    ingate_weight,
    forget_weight,
    ingate_bias,
    forget_bias,
    forget_slope,
    head_gain,
    output_weight,
):
    devices = lax.axis_size("tp")
    split_count = devices // HEADS
    own_index = lax.axis_index("tp")
    head_id = own_index // split_count
    onehot = (jnp.arange(HEADS) == head_id).astype(jnp.float32)
    position = lengths.astype(jnp.float32) / MAXLEN
    current = tokens
    memories, sums_list, stabs = ([], [], [])
    for block_id in range(cell_memory.shape[0]):
        gathered_rows = lax.all_gather(current, "tp", axis=1, tiled=True)
        row_float = gathered_rows.astype(jnp.float32)
        normed = (
            row_float
            * lax.rsqrt(jnp.mean(row_float * row_float, axis=-1, keepdims=True) + EPS)
            * norm_gain[block_id].astype(jnp.float32)
        ).astype(jnp.bfloat16)
        queries = jnp.dot(
            normed, query_weight[block_id], preferred_element_type=jnp.float32
        ).astype(jnp.bfloat16)
        key_rows = (
            jnp.dot(normed, key_weight[block_id], preferred_element_type=jnp.float32)
            * HEAD ** (-0.5)
        ).astype(jnp.bfloat16)
        values = jnp.dot(normed, value_weight[block_id], preferred_element_type=jnp.float32).astype(
            jnp.bfloat16
        )
        outgate = jnp.dot(
            normed, outgate_weight[block_id], preferred_element_type=jnp.float32
        ).astype(jnp.bfloat16)
        ingate = (
            jnp.dot(normed, ingate_weight[block_id], preferred_element_type=jnp.float32)
            + ingate_bias[block_id]
        )
        forget = jax.nn.log_sigmoid(
            jnp.dot(normed, forget_weight[block_id], preferred_element_type=jnp.float32)
            + forget_bias[block_id]
            + forget_slope[block_id] * position[:, None]
        )
        stab_new = jnp.maximum(forget + stabilizer[block_id], ingate)
        decays = jnp.exp(forget + stabilizer[block_id] - stab_new)
        in_weight = jnp.exp(ingate - stab_new)
        decay_own = jnp.sum(decays * onehot, axis=1)
        inweight_own = jnp.sum(in_weight * onehot, axis=1)
        sums_new = decay_own[:, None] * key_sums[block_id] + inweight_own[
            :, None
        ] * key_rows.astype(jnp.float32)
        head_pair = jnp.stack((queries, key_rows))
        head_sums = sums_new
        for level in range(split_count.bit_length() - 1):
            partner = from_partner(head_pair, "tp", level)
            upper = own_index // (1 << level) % 2 == 1
            lower_half = jnp.where(upper, partner, head_pair)
            upper_half = jnp.where(upper, head_pair, partner)
            head_pair = jnp.concatenate((lower_half, upper_half), axis=2)
            sums_mate = from_partner(head_sums, "tp", level)
            sums_low = jnp.where(upper, sums_mate, head_sums)
            sums_high = jnp.where(upper, head_sums, sums_mate)
            head_sums = jnp.concatenate((sums_low, sums_high), axis=1)
        head_query = head_pair[0].astype(jnp.float32)
        head_keys = head_pair[1].astype(jnp.float32)
        mem_new = (
            decay_own[:, None, None] * cell_memory[block_id]
            + inweight_own[:, None, None]
            * values.astype(jnp.float32)[:, :, None]
            * head_keys[:, None, :]
        )
        numerator = jnp.einsum("bvk,bk->bv", mem_new, head_query, precision=lax.Precision.HIGHEST)
        denominator = jnp.maximum(jnp.abs(jnp.sum(head_sums * head_query, axis=1)), 1.0)
        hidden = numerator / denominator[:, None]
        gated_out = (
            hidden
            * head_gain[block_id].astype(jnp.float32)
            * jax.nn.sigmoid(outgate.astype(jnp.float32))
        ).astype(jnp.bfloat16)
        out_weight = output_weight[block_id]
        projected = jnp.dot(
            lax.all_gather(gated_out, "tp", axis=1, tiled=True),
            out_weight,
            preferred_element_type=jnp.float32,
        )
        current = (current.astype(jnp.float32) + projected).astype(jnp.bfloat16)
        memories.append(mem_new)
        sums_list.append(sums_new)
        stabs.append(stab_new)
    return (current, jnp.stack(memories), jnp.stack(sums_list), jnp.stack(stabs))


def solution(mesh):
    in_specs = (
        P("grp", "tp"),
        P("grp"),
        P(None, "grp", "tp", None),
        P(None, "grp", "tp"),
        P(None, "grp", None),
        P(),
        P(None, None, "tp"),
        P(None, None, "tp"),
        P(None, None, "tp"),
        P(None, None, "tp"),
        P(),
        P(),
        P(),
        P(),
        P(),
        P(None, "tp"),
        P(None, None, "tp"),
    )
    out_specs = (
        P("grp", "tp"),
        P(None, "grp", "tp", None),
        P(None, "grp", "tp"),
        P(None, "grp", None),
    )
    return jax.shard_map(body, mesh=mesh, in_specs=in_specs, out_specs=out_specs, check_vma=False)
```

profile of v0, /device:TPU:0, one launch (start us, length us, event | category | flops | bytes accessed | tf_op | source)
XLA Modules:
  0.0 133.5 jit_solution(18110746305476406706)
XLA Ops:
  0.7 0.7 convert_multiply_fusion.4
  1.3 0.8 slice_bitcast_fusion
  2.1 0.8 slice_convert_fusion
  2.9 24.3 %all_gather.12 = bf16[80,2048]{1,0:T(8,128)(2,1)S(1)} all-gather(bf16[80,128]{1,0:T(8,128)(2,1)} %param.17), channel_id=1, replica_groups=mesh['grp'=2,'tp'=16] {'tp'}, dimensions={1}, use_global_device_ids=true | all-gather | bytes 348160 | tf_op jit(solution)/shard_map/all_gather | solution.py:46
  27.3 0.8 slice_bitcast_fusion.1
  28.1 1.3 %fusion.38 = bf16[1,80,128]{2,1,0:T(8,128)(2,1)S(1)} fusion(bf16[2,2048,128]{2,1,0:T(8,128)(2,1)} %param.23, bf16[80,2048]{1,0:T(8,128)(2,1)S(1)} %all_gather.12, f32[2048]{0:T(1024)S(1)} %bitcast.144, f32[80]{0:T(128)S(1)} %add_rsqrt_fusion.1), kind=kOutput, calls=%fused_computation.51 | convolution fusion | flops 42608640 | bytes 880960 | tf_op jit(solution)/shard_map/dot_general | solution.py:53
  29.4 1.1 fusion.93
  30.6 1.1 multiply_reduce_fusion.3
  31.7 1.4 %fusion.81 = (f32[80,128]{1,0:T(8,128)S(1)}, bf16[80,128]{1,0:T(8,128)(2,1)S(1)}) fusion(f32[2,80,128]{2,1,0:T(8,128)} %param.20, f32[80]{0:T(128)S(1)} %get-tuple-element.6, f32[80]{0:T(128)S(1)} %get-tuple-element.7, bf16[2,2048,128]{2,1,0:T(8,128)(2,1)} %param.24, bf16[80,2048]{1,0:T(8,128)(2,1)S(1)} %all_gather.12, f32[2048]{0:T(1024)S(1)} %bitcast.147, ...), kind=kOutput, calls=%fused_computation.115 | convolution fusion | flops 42659840 | bytes 963520 | tf_op jit(solution)/shard_map/dot_general | solution.py:57
  33.1 0.4 collective-permute-start
  33.5 0.2 collective-permute-start.1
  33.7 1.3 %fusion.37 = f32[80,128]{1,0:T(8,128)S(1)} fusion(bf16[2,2048,128]{2,1,0:T(8,128)(2,1)} %param.25, f32[80]{0:T(128)S(1)} %get-tuple-element.7, bf16[80,2048]{1,0:T(8,128)(2,1)S(1)} %all_gather.12, f32[2048]{0:T(1024)S(1)} %bitcast.148, f32[80]{0:T(128)S(1)} %add_rsqrt_fusion.1), kind=kOutput, calls=%fused_computation.50 | convolution fusion | flops 42629120 | bytes 901760 | tf_op jit(solution)/shard_map/dot_general | solution.py:60
  35.0 0.7 bitcast_convert_fusion
  36.0 8.7 %fusion.4 = f32[80,1,128]{2,1,0:T(1,128)S(1)} fusion(f32[2,80,128,256]{3,2,1,0:T(8,128)} %param.19, f32[80,256]{1,0:T(8,128)S(1)} %get-tuple-element.19, f32[80,128]{1,0:T(8,128)S(1)} %fusion.37, f32[80]{0:T(128)S(1)} %get-tuple-element.6, bf16[80,256,1]{1,0,2:T(8,128)(2,1)S(1)} %get-tuple-element.18), kind=kOutput, calls=%fused_computation.6 | convolution fusion | flops 39321600 | bytes 10690880 | tf_op jit(solution)/shard_map/bvk,bk->bv/dot_general | solution.py:103
  44.7 0.3 fusion.35
  45.0 18.3 %all_gather.13 = bf16[80,2048]{1,0:T(8,128)(2,1)S(1)} all-gather(bf16[80,128]{1,0:T(8,128)(2,1)S(1)} %fusion.35), channel_id=1, replica_groups=mesh['grp'=2,'tp'=16] {'tp'}, dimensions={1}, use_global_device_ids=true | all-gather | bytes 348160 | tf_op jit(solution)/shard_map/all_gather | solution.py:113
  63.3 0.2 fusion.17
  63.6 19.7 %all_gather.14 = bf16[80,2048]{1,0:T(8,128)(2,1)S(1)} all-gather(bf16[80,128]{1,0:T(8,128)(2,1)S(1)} %fusion.17), channel_id=1, replica_groups=mesh['grp'=2,'tp'=16] {'tp'}, dimensions={1}, use_global_device_ids=true | all-gather | bytes 348160 | tf_op jit(solution)/shard_map/all_gather | solution.py:46
  83.4 0.3 fusion.39
  83.8 0.3 fusion.95
  84.1 0.3 multiply_reduce_fusion.1
  84.4 0.3 fusion.28
  84.7 0.3 fusion.80
  85.0 0.4 collective-permute-start.2
  85.6 0.6 pad_maximum_fusion.1
  86.3 0.6 pad_maximum_fusion.6
  87.1 10.3 %multiply_add_fusion.1 = (f32[1,80,128,256]{3,2,1,0:T(8,128)S(1)}, f32[1,80,128,256]{3,2,1,0:T(8,128)S(1)}) fusion(f32[2,80,128,256]{3,2,1,0:T(8,128)} %param.19, f32[80,256]{1,0:T(8,128)S(1)} %get-tuple-element.19, f32[80,128]{1,0:T(8,128)S(1)} %fusion.37, f32[80]{0:T(128)S(1)} %get-tuple-element.6, f32[80,256]{1,0:T(8,128)S(1)} %get-tuple-element.13, ...), kind=kLoop, calls=%fused_computation.8 | loop fusion | flops 15728640 | bytes 42189440 | tf_op jit(solution)/shard_map/add | solution.py:98
  97.4 8.6 %fusion.1 = f32[80,1,128]{2,1,0:T(1,128)S(1)} fusion(f32[2,80,128,256]{3,2,1,0:T(8,128)} %param.19, f32[80,256]{1,0:T(8,128)S(1)} %get-tuple-element.13, f32[80,128]{1,0:T(8,128)S(1)} %fusion.28, f32[80]{0:T(128)S(1)} %get-tuple-element.4, bf16[80,256,1]{1,0,2:T(8,128)(2,1)S(1)} %get-tuple-element.12), kind=kOutput, calls=%fused_computation.3 | convolution fusion | flops 39321600 | bytes 10690880 | tf_op jit(solution)/shard_map/bvk,bk->bv/dot_general | solution.py:103
  106.0 0.3 fusion.26
  106.3 18.3 %all_gather.15 = bf16[80,2048]{1,0:T(8,128)(2,1)S(1)} all-gather(bf16[80,128]{1,0:T(8,128)(2,1)S(1)} %fusion.26), channel_id=1, replica_groups=mesh['grp'=2,'tp'=16] {'tp'}, dimensions={1}, use_global_device_ids=true | all-gather | bytes 348160 | tf_op jit(solution)/shard_map/all_gather | solution.py:113
  124.6 0.9 fusion.19
  125.5 8.0 %pad_maximum_fusion = f32[2,80,128,256]{3,2,1,0:T(8,128)} fusion(f32[1,80,128,256]{3,2,1,0:T(8,128)S(1)} %get-tuple-element.9, f32[1,80,128,256]{3,2,1,0:T(8,128)S(1)} %get-tuple-element.8), kind=kLoop, calls=%fused_computation | loop fusion | flops 5242880 | bytes 41943040 | tf_op jit(solution)/shard_map/stack | solution.py:121
  (42 shorter events, 0.9 us)
Async XLA Ops:
  27.1 36.2 %copy-start = (bf16[80,128]{1,0:T(8,128)(2,1)S(1)}, bf16[80,128]{1,0:T(8,128)(2,1)}, u32[]{:S(2)}) copy-start(bf16[80,128]{1,0:T(8,128)(2,1)} %param.17) | copy-start | bytes 61444
  29.4 54.0 %copy-start.1 = (bf16[2,2048,128]{2,1,0:T(8,128)(2,1)S(1)}, bf16[2,2048,128]{2,1,0:T(8,128)(2,1)}, u32[]{:S(2)}) copy-start(bf16[2,2048,128]{2,1,0:T(8,128)(2,1)} %param.23) | copy-start | bytes 3145732
  31.6 52.1 %copy-start.7 = (bf16[2,2048,8]{1,2,0:T(8,128)(2,1)S(1)}, bf16[2,2048,8]{1,2,0:T(8,128)(2,1)}, u32[]{:S(2)}) copy-start(bf16[2,2048,8]{1,2,0:T(8,128)(2,1)} %param.28) | copy-start | bytes 196612
  31.6 52.1 %copy-start.9 = (f32[2,80,8]{1,2,0:T(8,128)S(1)}, f32[2,80,8]{1,2,0:T(8,128)}, u32[]{:S(2)}) copy-start(f32[2,80,8]{1,2,0:T(8,128)} %param.21) | copy-start | bytes 15364
  31.7 52.4 %copy-start.8 = (bf16[2,2048,8]{1,2,0:T(8,128)(2,1)S(1)}, bf16[2,2048,8]{1,2,0:T(8,128)(2,1)}, u32[]{:S(2)}) copy-start(bf16[2,2048,8]{1,2,0:T(8,128)(2,1)} %param.27) | copy-start | bytes 196612
  33.1 51.3 %copy-start.2 = (bf16[2,2048,128]{2,1,0:T(8,128)(2,1)S(1)}, bf16[2,2048,128]{2,1,0:T(8,128)(2,1)}, u32[]{:S(2)}) copy-start(bf16[2,2048,128]{2,1,0:T(8,128)(2,1)} %param.25) | copy-start | bytes 3145732
  33.1 2.7 %collective-permute-start = (bf16[2,80,128]{2,1,0:T(8,128)(2,1)S(1)}, bf16[2,80,128]{2,1,0:T(8,128)(2,1)S(1)}, u32[]{:S(2)}, u32[]{:S(2)}) collective-permute-start(bf16[2,80,128]{2,1,0:T(8,128)(2,1)S(1)} %pad_maximum_fusion.4), channel_id=1, source_target_pairs={{0,1},{1,0},{2,3},{3,2},{4,5},{5,4},{6,7},{7,6},{8,9},{9,8},{10,11... | collective-permute-start | bytes 122888 | tf_op jit(solution)/shard_map/ppermute | solution.py:15
  33.5 2.3 %collective-permute-start.1 = (f32[80,128]{1,0:T(8,128)S(1)}, f32[80,128]{1,0:T(8,128)S(1)}, u32[]{:S(2)}, u32[]{:S(2)}) collective-permute-start(f32[80,128]{1,0:T(8,128)S(1)} %get-tuple-element.34), channel_id=1, source_target_pairs={{0,1},{1,0},{2,3},{3,2},{4,5},{5,4},{6,7},{7,6},{8,9},{9,8},{10,11... | collective-permute-start | bytes 122888 | tf_op jit(solution)/shard_map/ppermute | solution.py:15
  35.0 49.7 %copy-start.6 = (f32[2,80,128]{2,1,0:T(8,128)S(1)}, f32[2,80,128]{2,1,0:T(8,128)}, u32[]{:S(2)}) copy-start(f32[2,80,128]{2,1,0:T(8,128)} %param.20) | copy-start | bytes 245764
  35.8 8.9 %copy-start.4 = (bf16[2,2048,128]{2,1,0:T(8,128)(2,1)S(1)}, bf16[2,2048,128]{2,1,0:T(8,128)(2,1)}, u32[]{:S(2)}) copy-start(bf16[2,2048,128]{2,1,0:T(8,128)(2,1)} %param.26) | copy-start | bytes 3145732
  35.8 27.6 %copy-start.5 = (bf16[2,2048,128]{2,1,0:T(8,128)(2,1)S(1)}, bf16[2,2048,128]{2,1,0:T(8,128)(2,1)}, u32[]{:S(2)}) copy-start(bf16[2,2048,128]{2,1,0:T(8,128)(2,1)} %param.33) | copy-start | bytes 3145732
  35.8 48.9 %copy-start.3 = (bf16[2,2048,128]{2,1,0:T(8,128)(2,1)S(1)}, bf16[2,2048,128]{2,1,0:T(8,128)(2,1)}, u32[]{:S(2)}) copy-start(bf16[2,2048,128]{2,1,0:T(8,128)(2,1)} %param.24) | copy-start | bytes 3145732
  85.0 1.8 %collective-permute-start.2 = (bf16[2,80,128]{2,1,0:T(8,128)(2,1)S(1)}, bf16[2,80,128]{2,1,0:T(8,128)(2,1)S(1)}, u32[]{:S(2)}, u32[]{:S(2)}) collective-permute-start(bf16[2,80,128]{2,1,0:T(8,128)(2,1)S(1)} %pad_maximum_fusion.5), channel_id=1, source_target_pairs={{0,1},{1,0},{2,3},{3,2},{4,5},{5,4},{6,7},{7,6},{8,9},{9,8},{10,11... | collective-permute-start | bytes 122888 | tf_op jit(solution)/shard_map/ppermute | solution.py:15
  85.5 1.4 %collective-permute-start.3 = (f32[80,128]{1,0:T(8,128)S(1)}, f32[80,128]{1,0:T(8,128)S(1)}, u32[]{:S(2)}, u32[]{:S(2)}) collective-permute-start(f32[80,128]{1,0:T(8,128)S(1)} %get-tuple-element.36), channel_id=1, source_target_pairs={{0,1},{1,0},{2,3},{3,2},{4,5},{5,4},{6,7},{7,6},{8,9},{9,8},{10,11... | collective-permute-start | bytes 122888 | tf_op jit(solution)/shard_map/ppermute | solution.py:15
where the time goes:
time: 134 us; the launch traced here: 133 us
  blocking collectives  80.6 us (60%)
  matrix products  26.8 us (20%)
  other arithmetic  22.4 us (17%)
  local copies, waits for them, and re-layouts  1.58 us (1%)
    all_gather x2, blocking collectives, body(): gathered_rows = lax.all_gather(current, 'tp', axis=1, tiled=True)  43.9 us
    all_gather x2, blocking collectives, body(): lax.all_gather(gated_out, 'tp', axis=1, tiled=True)  36.7 us
    dot_general x2, matrix products, body(): jnp.einsum('bvk,bk->bv', mem_new, head_query, precision=lax.Precision.HIG...  17.2 us
    add x1, other arithmetic, body(): decay_own[:, None, None] * cell_memory[block_id]  10.3 us
    another operation x1, other arithmetic, body(): jnp.stack(memories)  8 us
  transfers between devices with their start and end apart: 4, of which 0 were waited for; matrix products, arithmetic and copies ran while one was open for 3% of the time, Pallas kernels for 0%

commit v1 on v0

--- a/solution.py
+++ b/solution.py
@@ -43,7 +43,7 @@
     current = tokens
     memories, sums_list, stabs = ([], [], [])
     for block_id in range(cell_memory.shape[0]):
-        gathered_rows = lax.all_gather(current, "tp", axis=1, tiled=True)
+        gathered_rows = jnp.concatenate(lax.all_gather(current, "tp"), axis=1)
         row_float = gathered_rows.astype(jnp.float32)
         normed = (
             row_float

time: 134 us -> 134 us (level)
  transfers between devices with their start and end apart: 4 -> 4, of which waited for: 0 -> 0; matrix products, arithmetic and copies ran while one was open for 3% -> 2% of each run, Pallas kernels for 0% -> 0%
where the time goes in v1:
time: 134 us; the launch traced here: 133 us
  blocking collectives  80.6 us (60%)
  matrix products  26 us (19%)
  other arithmetic  23.1 us (17%)
  local copies, waits for them, and re-layouts  1.57 us (1%)
    all_gather x2, blocking collectives, body(): gathered_rows = jnp.concatenate(lax.all_gather(current, 'tp'), axis=1)  43.9 us
    all_gather x2, blocking collectives, body(): lax.all_gather(gated_out, 'tp', axis=1, tiled=True)  36.7 us
    dot_general x2, matrix products, body(): jnp.einsum('bvk,bk->bv', mem_new, head_query, precision=lax.Precision.HIG...  17.2 us
    add x1, other arithmetic, body(): decay_own[:, None, None] * cell_memory[block_id]  10.4 us
    another operation x1, other arithmetic, body(): jnp.stack(memories)  8 us
  transfers between devices with their start and end apart: 4, of which 0 were waited for; matrix products, arithmetic and copies ran while one was open for 2% of the time, Pallas kernels for 0%

profile of v1, /device:TPU:0, one launch (start us, length us, event | category | flops | bytes accessed | tf_op | source)
XLA Modules:
  0.0 133.4 jit_solution(5327422206133025960)
XLA Ops:
  0.6 24.3 %all-gather = bf16[1280,128]{1,0:T(8,128)(2,1)S(1)} all-gather(bf16[80,128]{1,0:T(8,128)(2,1)} %param.17), channel_id=2, replica_groups=mesh['grp'=2,'tp'=16] {'tp'}, dimensions={0}, use_global_device_ids=true | all-gather | bytes 348160 | tf_op jit(solution)/shard_map/all_gather | solution.py:46
  25.2 0.7 convert_multiply_fusion
  25.8 0.8 slice_bitcast_fusion
  26.6 0.8 slice_convert_fusion
  27.4 0.8 slice_bitcast_fusion.1
  28.1 0.3 fusion.47
  28.4 1.3 fusion.38
  29.7 1.0 fusion.115
  30.7 1.0 multiply_reduce_fusion.5
  31.7 1.4 %fusion.103 = (f32[80,128]{1,0:T(8,128)S(1)}, bf16[80,128]{1,0:T(8,128)(2,1)S(1)}) fusion(f32[2,80,128]{2,1,0:T(8,128)} %param.20, f32[80]{0:T(128)S(1)} %get-tuple-element.6, f32[80]{0:T(128)S(1)} %get-tuple-element.7, bf16[2,2048,128]{2,1,0:T(8,128)(2,1)} %param.24, bf16[10,8,16,128]{3,2,1,0:T(8,128)(2,1)S(1)} %bitcast.191), kind=kOutput, calls=%fused_computation.137 | convolution fusion | flops 42004480 | bytes 955008 | tf_op jit(solution)/shard_map/dot_general | solution.py:57
  33.1 0.4 collective-permute-start
  33.7 1.3 fusion.37
  35.0 0.8 bitcast_convert_fusion
  36.0 8.7 %fusion.4 = f32[80,1,128]{2,1,0:T(1,128)S(1)} fusion(f32[2,80,128,256]{3,2,1,0:T(8,128)} %param.19, f32[80,256]{1,0:T(8,128)S(1)} %get-tuple-element.19, f32[80,128]{1,0:T(8,128)S(1)} %fusion.37, f32[80]{0:T(128)S(1)} %get-tuple-element.6, bf16[80,256,1]{1,0,2:T(8,128)(2,1)S(1)} %get-tuple-element.18), kind=kOutput, calls=%fused_computation.6 | convolution fusion | flops 39321600 | bytes 10690880 | tf_op jit(solution)/shard_map/bvk,bk->bv/dot_general | solution.py:103
  44.7 0.3 fusion.35
  44.9 18.3 %all_gather.20 = bf16[80,2048]{1,0:T(8,128)(2,1)S(1)} all-gather(bf16[80,128]{1,0:T(8,128)(2,1)S(1)} %fusion.35), channel_id=1, replica_groups=mesh['grp'=2,'tp'=16] {'tp'}, dimensions={1}, use_global_device_ids=true | all-gather | bytes 348160 | tf_op jit(solution)/shard_map/all_gather | solution.py:113
  63.3 0.2 fusion.17
  63.5 19.7 %all-gather.1 = bf16[1280,128]{1,0:T(8,128)(2,1)S(1)} all-gather(bf16[80,128]{1,0:T(8,128)(2,1)S(1)} %fusion.17), channel_id=3, replica_groups=mesh['grp'=2,'tp'=16] {'tp'}, dimensions={0}, use_global_device_ids=true | all-gather | bytes 348160 | tf_op jit(solution)/shard_map/all_gather | solution.py:46
  83.4 0.3 fusion.45
  83.7 0.2 fusion.39
  84.2 0.2 multiply_reduce_fusion.3
  84.4 0.2 fusion.28
  84.7 0.2 fusion.102
  85.0 0.4 collective-permute-start.2
  85.5 0.6 pad_maximum_fusion.1
  86.2 0.6 pad_maximum_fusion.6
  87.0 10.4 %multiply_add_fusion.1 = (f32[1,80,128,256]{3,2,1,0:T(8,128)S(1)}, f32[1,80,128,256]{3,2,1,0:T(8,128)S(1)}) fusion(f32[2,80,128,256]{3,2,1,0:T(8,128)} %param.19, f32[80,256]{1,0:T(8,128)S(1)} %get-tuple-element.19, f32[80,128]{1,0:T(8,128)S(1)} %fusion.37, f32[80]{0:T(128)S(1)} %get-tuple-element.6, f32[80,256]{1,0:T(8,128)S(1)} %get-tuple-element.13, ...), kind=kLoop, calls=%fused_computation.8 | loop fusion | flops 15728640 | bytes 42189440 | tf_op jit(solution)/shard_map/add | solution.py:98
  97.3 8.6 %fusion.1 = f32[80,1,128]{2,1,0:T(1,128)S(1)} fusion(f32[2,80,128,256]{3,2,1,0:T(8,128)} %param.19, f32[80,256]{1,0:T(8,128)S(1)} %get-tuple-element.13, f32[80,128]{1,0:T(8,128)S(1)} %fusion.28, f32[80]{0:T(128)S(1)} %get-tuple-element.4, bf16[80,256,1]{1,0,2:T(8,128)(2,1)S(1)} %get-tuple-element.12), kind=kOutput, calls=%fused_computation.3 | convolution fusion | flops 39321600 | bytes 10690880 | tf_op jit(solution)/shard_map/bvk,bk->bv/dot_general | solution.py:103
  105.9 0.3 fusion.26
  106.2 18.3 %all_gather.23 = bf16[80,2048]{1,0:T(8,128)(2,1)S(1)} all-gather(bf16[80,128]{1,0:T(8,128)(2,1)S(1)} %fusion.26), channel_id=1, replica_groups=mesh['grp'=2,'tp'=16] {'tp'}, dimensions={1}, use_global_device_ids=true | all-gather | bytes 348160 | tf_op jit(solution)/shard_map/all_gather | solution.py:113
  124.5 0.9 fusion.19
  125.4 8.0 %pad_maximum_fusion = f32[2,80,128,256]{3,2,1,0:T(8,128)} fusion(f32[1,80,128,256]{3,2,1,0:T(8,128)S(1)} %get-tuple-element.9, f32[1,80,128,256]{3,2,1,0:T(8,128)S(1)} %get-tuple-element.8), kind=kLoop, calls=%fused_computation | loop fusion | flops 5242880 | bytes 41943040 | tf_op jit(solution)/shard_map/stack | solution.py:121
  (46 shorter events, 1.3 us)
Async XLA Ops:
  25.1 38.2 %copy-start = (bf16[80,128]{1,0:T(8,128)(2,1)S(1)}, bf16[80,128]{1,0:T(8,128)(2,1)}, u32[]{:S(2)}) copy-start(bf16[80,128]{1,0:T(8,128)(2,1)} %param.17) | copy-start | bytes 61444
  31.7 52.0 %copy-start.1 = (bf16[2,2048,128]{2,1,0:T(8,128)(2,1)S(1)}, bf16[2,2048,128]{2,1,0:T(8,128)(2,1)}, u32[]{:S(2)}) copy-start(bf16[2,2048,128]{2,1,0:T(8,128)(2,1)} %param.23) | copy-start | bytes 3145732
  33.1 2.7 %collective-permute-start = (bf16[2,80,128]{2,1,0:T(8,128)(2,1)S(1)}, bf16[2,80,128]{2,1,0:T(8,128)(2,1)S(1)}, u32[]{:S(2)}, u32[]{:S(2)}) collective-permute-start(bf16[2,80,128]{2,1,0:T(8,128)(2,1)S(1)} %pad_maximum_fusion.4), channel_id=1, source_target_pairs={{0,1},{1,0},{2,3},{3,2},{4,5},{5,4},{6,7},{7,6},{8,9},{9,8},{10,11... | collective-permute-start | bytes 122888 | tf_op jit(solution)/shard_map/ppermute | solution.py:15
  33.5 50.5 %copy-start.7 = (bf16[2,2048,8]{1,2,0:T(8,128)(2,1)S(1)}, bf16[2,2048,8]{1,2,0:T(8,128)(2,1)}, u32[]{:S(2)}) copy-start(bf16[2,2048,8]{1,2,0:T(8,128)(2,1)} %param.28) | copy-start | bytes 196612
  33.5 50.5 %copy-start.9 = (f32[2,80,8]{1,2,0:T(8,128)S(1)}, f32[2,80,8]{1,2,0:T(8,128)}, u32[]{:S(2)}) copy-start(f32[2,80,8]{1,2,0:T(8,128)} %param.21) | copy-start | bytes 15364
  33.5 2.3 %collective-permute-start.1 = (f32[80,128]{1,0:T(8,128)S(1)}, f32[80,128]{1,0:T(8,128)S(1)}, u32[]{:S(2)}, u32[]{:S(2)}) collective-permute-start(f32[80,128]{1,0:T(8,128)S(1)} %get-tuple-element.34), channel_id=1, source_target_pairs={{0,1},{1,0},{2,3},{3,2},{4,5},{5,4},{6,7},{7,6},{8,9},{9,8},{10,11... | collective-permute-start | bytes 122888 | tf_op jit(solution)/shard_map/ppermute | solution.py:15
  34.9 49.2 %copy-start.8 = (bf16[2,2048,8]{1,2,0:T(8,128)(2,1)S(1)}, bf16[2,2048,8]{1,2,0:T(8,128)(2,1)}, u32[]{:S(2)}) copy-start(bf16[2,2048,8]{1,2,0:T(8,128)(2,1)} %param.27) | copy-start | bytes 196612
  35.0 49.5 %copy-start.2 = (bf16[2,2048,128]{2,1,0:T(8,128)(2,1)S(1)}, bf16[2,2048,128]{2,1,0:T(8,128)(2,1)}, u32[]{:S(2)}) copy-start(bf16[2,2048,128]{2,1,0:T(8,128)(2,1)} %param.25) | copy-start | bytes 3145732
  35.7 8.9 %copy-start.4 = (bf16[2,2048,128]{2,1,0:T(8,128)(2,1)S(1)}, bf16[2,2048,128]{2,1,0:T(8,128)(2,1)}, u32[]{:S(2)}) copy-start(bf16[2,2048,128]{2,1,0:T(8,128)(2,1)} %param.26) | copy-start | bytes 3145732
  35.7 27.5 %copy-start.5 = (bf16[2,2048,128]{2,1,0:T(8,128)(2,1)S(1)}, bf16[2,2048,128]{2,1,0:T(8,128)(2,1)}, u32[]{:S(2)}) copy-start(bf16[2,2048,128]{2,1,0:T(8,128)(2,1)} %param.33) | copy-start | bytes 3145732
  35.9 48.7 %copy-start.3 = (bf16[2,2048,128]{2,1,0:T(8,128)(2,1)S(1)}, bf16[2,2048,128]{2,1,0:T(8,128)(2,1)}, u32[]{:S(2)}) copy-start(bf16[2,2048,128]{2,1,0:T(8,128)(2,1)} %param.24) | copy-start | bytes 3145732
  35.9 48.7 %copy-start.6 = (f32[2,80,128]{2,1,0:T(8,128)S(1)}, f32[2,80,128]{2,1,0:T(8,128)}, u32[]{:S(2)}) copy-start(f32[2,80,128]{2,1,0:T(8,128)} %param.20) | copy-start | bytes 245764
  85.0 1.8 %collective-permute-start.2 = (bf16[2,80,128]{2,1,0:T(8,128)(2,1)S(1)}, bf16[2,80,128]{2,1,0:T(8,128)(2,1)S(1)}, u32[]{:S(2)}, u32[]{:S(2)}) collective-permute-start(bf16[2,80,128]{2,1,0:T(8,128)(2,1)S(1)} %pad_maximum_fusion.5), channel_id=1, source_target_pairs={{0,1},{1,0},{2,3},{3,2},{4,5},{5,4},{6,7},{7,6},{8,9},{9,8},{10,11... | collective-permute-start | bytes 122888 | tf_op jit(solution)/shard_map/ppermute | solution.py:15
  85.4 1.4 %collective-permute-start.3 = (f32[80,128]{1,0:T(8,128)S(1)}, f32[80,128]{1,0:T(8,128)S(1)}, u32[]{:S(2)}, u32[]{:S(2)}) collective-permute-start(f32[80,128]{1,0:T(8,128)S(1)} %get-tuple-element.36), channel_id=1, source_target_pairs={{0,1},{1,0},{2,3},{3,2},{4,5},{5,4},{6,7},{7,6},{8,9},{9,8},{10,11... | collective-permute-start | bytes 122888 | tf_op jit(solution)/shard_map/ppermute | solution.py:15
